TPU v7x, 512 devices: a whole 4x4x16 slice. The times are simulated.
512 devices in a mesh: sp: 256 (over z, y, x), tp: 2 (over core).
Axes of the slice: x: 4, y: 4, z: 16, core: 2. Of those that a mesh axis runs over, the one named last changes fastest.
Arguments:
- query_rows: bfloat16 [65536, 1024], P('sp', 'tp'), may hold values from -6 to 6
- key_rows: bfloat16 [65536, 1024], P('sp', 'tp'), may hold values from -6 to 6
- value_rows: bfloat16 [65536, 1024], P('sp', 'tp'), may hold values from -6 to 6
- out_weight: bfloat16 [1024, 2048], P('tp'), may hold values from -0.75 to 0.75
Outputs:
- layer_out: bfloat16 [65536, 2048], P(('sp', 'tp'))
All inputs are finite; a program needn't handle non-finite values.
Results may differ from a plain program's by a relative error of at most 0.012.
Values may be sent and summed in bfloat16 or wider, within the bound.
No kernel may reach another device: no remote copies, remote signals or barrier semaphores. Data moves between devices by JAX's collectives and lax.ppermute only.
A program may use at most 64 MiB of HBM per device.

v0:
```python
import math
import jax
import jax.numpy as jnp
from jax import lax
from jax.sharding import PartitionSpec as P

HD = 64
BACK = 128
THETA = 500000.0
DILATIONS = (1, 4, 16)


def shifted(value, axis, steps):
    count = lax.axis_size(axis)
    initial, last = (max(0, -steps), min(count, count - steps))
    return lax.ppermute(value, axis, [(source, source + steps) for source in range(initial, last)])


def rotate(rows, positions, head_count, head_dim):
    half_dim = head_dim // 2
    inverse = jnp.power(jnp.float32(THETA), -jnp.arange(half_dim, dtype=jnp.float32) / half_dim)
    angles = positions.astype(jnp.float32)[:, None] * inverse[None, :]
    cosine = jnp.cos(angles)[:, None, :]
    sine = jnp.sin(angles)[:, None, :]
    whole = rows.astype(jnp.float32).reshape(rows.shape[0], head_count, head_dim)
    lower = whole[..., :half_dim]
    upper = whole[..., half_dim:]
    turned = jnp.concatenate(
        [lower * cosine - upper * sine, upper * cosine + lower * sine], axis=-1
    )
    return turned.reshape(rows.shape[0], head_count * head_dim).astype(jnp.bfloat16)


def pattern_part(queries, key_ext, value_ext, dilation, anchor, head_count):
    tok_rows = queries.shape[0]
    length = tok_rows // dilation
    nblocks = max(1, length // BACK)
    block_rows = length // nblocks
    query_sub = queries.reshape(length, dilation, head_count, HD)
    key_sub = key_ext.reshape(BACK + length, dilation, head_count, HD)
    value_sub = value_ext.reshape(BACK + length, dilation, head_count, HD)
    residues = jnp.arange(dilation, dtype=jnp.int32)[:, None, None, None]
    results, maxima, sums = ([], [], [])
    for block_index in range(nblocks):
        first_row = block_index * block_rows
        key_part = key_sub[first_row : first_row + BACK + block_rows]
        value_part = value_sub[first_row : first_row + BACK + block_rows]
        scores = jnp.einsum(
            "qrhc,krhc->rhqk",
            query_sub[first_row : first_row + block_rows],
            key_part,
            preferred_element_type=jnp.float32,
        ) * (1.0 / math.sqrt(HD))
        query_index = jnp.arange(block_rows, dtype=jnp.int32)[:, None]
        key_index = jnp.arange(BACK + block_rows, dtype=jnp.int32)[None, :]
        distance = query_index + BACK - key_index
        key_position = anchor + (first_row + key_index - BACK) * dilation + residues
        allowed = (distance >= 0) & (distance <= BACK) & (key_position >= 0)
        scores = jnp.where(allowed, scores, -jnp.inf)
        row_max = jnp.max(scores, axis=-1)
        weights = jnp.exp(scores - row_max[..., None])
        row_sum = jnp.sum(weights, axis=-1)
        weighted = jnp.einsum(
            "rhqk,krhc->qrhc",
            weights.astype(jnp.bfloat16),
            value_part,
            preferred_element_type=jnp.float32,
        )
        sum_rows = row_sum.transpose(2, 0, 1)
        results.append((weighted / sum_rows[..., None]).astype(jnp.bfloat16))
        maxima.append(row_max.transpose(2, 0, 1))
        sums.append(sum_rows)
    result = jnp.concatenate(results, axis=0).reshape(tok_rows, head_count, HD)
    row_max = jnp.concatenate(maxima, axis=0).reshape(tok_rows, head_count)
    row_sum = jnp.concatenate(sums, axis=0).reshape(tok_rows, head_count)
    return (result, row_max, row_sum)


def per_device(query_rows, key_rows, value_rows, out_weight):
    tok_rows = query_rows.shape[0]
    head_count = query_rows.shape[1] // HD
    anchor = lax.axis_index("sp") * tok_rows
    positions = anchor + jnp.arange(tok_rows, dtype=jnp.int32)
    turned_q = rotate(query_rows, positions, head_count, HD)
    turned_k = rotate(key_rows, positions, head_count, HD)
    paired = jnp.stack((turned_k, value_rows))
    pieces = -(-(16 * BACK) // tok_rows)
    held = paired
    gathered = 1
    while gathered < pieces + 1:
        needed = min(gathered, pieces + 1 - gathered)
        arrived = shifted(held[:, held.shape[1] - needed * tok_rows :], "sp", gathered)
        held = jnp.concatenate([arrived, held], axis=1)
        gathered = gathered + needed
    prior = held[:, : held.shape[1] - tok_rows]
    results, maxima, sums = ([], [], [])
    for dilation in DILATIONS:
        reach = BACK * dilation
        key_ext = jnp.concatenate([prior[0, prior.shape[1] - reach :], turned_k], axis=0)
        value_ext = jnp.concatenate([prior[1, prior.shape[1] - reach :], value_rows], axis=0)
        result, row_max, row_sum = pattern_part(
            turned_q, key_ext, value_ext, dilation, anchor, head_count
        )
        results.append(result)
        maxima.append(row_max)
        sums.append(row_sum)
    top = jnp.maximum(jnp.maximum(maxima[0], maxima[1]), maxima[2])
    scales = [sums[i] * jnp.exp(maxima[i] - top) for i in range(3)]
    weighted = scales[0][..., None] * results[0].astype(jnp.float32)
    weighted = weighted + scales[1][..., None] * results[1].astype(jnp.float32)
    weighted = weighted + scales[2][..., None] * results[2].astype(jnp.float32)
    denominator = scales[0] + scales[1] + scales[2]
    mixed = (
        (weighted / denominator[..., None]).reshape(tok_rows, head_count * HD).astype(jnp.bfloat16)
    )
    token_rows = lax.all_to_all(mixed, "tp", split_axis=0, concat_axis=1, tiled=True)
    projected = jnp.dot(
        token_rows,
        lax.all_gather(out_weight, "tp", axis=0, tiled=True),
        preferred_element_type=jnp.float32,
    )
    return projected.astype(jnp.bfloat16)


def solution(mesh):
    return jax.shard_map(
        per_device,
        mesh=mesh,
        in_specs=(P("sp", "tp"), P("sp", "tp"), P("sp", "tp"), P("tp", None)),
        out_specs=P(("sp", "tp"), None),
        check_vma=False,
    )
```

profile of v0, /device:TPU:259, one launch (start us, length us, event | category | flops | bytes accessed | tf_op | source)
XLA Modules:
  0.0 195.9 jit_solution(11508287023331739371)
XLA Ops:
  10.2 3.1 %collective-permute-start = (bf16[2,256,512]{2,1,0:T(8,128)(2,1)}, bf16[2,256,512]{2,1,0:T(8,128)(2,1)S(1)}, u32[]{:S(2)}, u32[]{:S(2)}) collective-permute-start(bf16[2,256,512]{2,1,0:T(8,128)(2,1)} %pad_maximum_fusion.4), channel_id=1, source_target_pairs={{0,2},{2,4},{4,6},{6,8},{8,10},{10,12},{12,14},{14,16},{16,18},{18... | collective-permute-start | bytes 1572872 | tf_op jit(solution)/shard_map/ppermute | solution.py:16
  13.3 4.8 %collective-permute-start.2 = (bf16[2,256,512]{2,1,0:T(8,128)(2,1)}, bf16[2,256,512]{2,1,0:T(8,128)(2,1)}, u32[]{:S(2)}, u32[]{:S(2)}) collective-permute-start(bf16[2,256,512]{2,1,0:T(8,128)(2,1)} %pad_maximum_fusion.4), channel_id=1, source_target_pairs={{0,16},{2,18},{4,20},{6,22},{8,24},{10,26},{12,28},{14,30},{16,32}... | collective-permute-start | bytes 1572872 | tf_op jit(solution)/shard_map/ppermute | solution.py:16
  20.3 4.9 %collective-permute-done = bf16[2,256,512]{2,1,0:T(8,128)(2,1)S(1)} collective-permute-done((bf16[2,256,512]{2,1,0:T(8,128)(2,1)}, bf16[2,256,512]{2,1,0:T(8,128)(2,1)S(1)}, u32[]{:S(2)}, u32[]{:S(2)}) %collective-permute-start) | collective-permute-done | bytes 524320 | tf_op jit(solution)/shard_map/ppermute | solution.py:16
  25.3 3.8 %collective-permute-start.1 = (bf16[2,512,512]{2,1,0:T(8,128)(2,1)S(1)}, bf16[2,512,512]{2,1,0:T(8,128)(2,1)S(1)}, u32[]{:S(2)}, u32[]{:S(2)}) collective-permute-start(bf16[2,512,512]{2,1,0:T(8,128)(2,1)S(1)} %maximum_maximum_fusion.1), channel_id=1, source_target_pairs={{0,4},{2,6},{4,8},{6,10},{8,12},{10,14},{12,16},{14,18},{16,20},{1... | collective-permute-start | bytes 3145736 | tf_op jit(solution)/shard_map/ppermute | solution.py:16
  30.1 36.6 %collective-permute-done.1 = bf16[2,512,512]{2,1,0:T(8,128)(2,1)S(1)} collective-permute-done((bf16[2,512,512]{2,1,0:T(8,128)(2,1)S(1)}, bf16[2,512,512]{2,1,0:T(8,128)(2,1)S(1)}, u32[]{:S(2)}, u32[]{:S(2)}) %collective-permute-start.1) | collective-permute-done | bytes 1048608 | tf_op jit(solution)/shard_map/ppermute | solution.py:16
  68.1 1.9 collective-permute-start.3
  80.1 39.1 %collective-permute-done.3 = bf16[2,1024,512]{2,1,0:T(8,128)(2,1)} collective-permute-done((bf16[2,1024,512]{2,1,0:T(8,128)(2,1)}, bf16[2,1024,512]{2,1,0:T(8,128)(2,1)}, u32[]{:S(2)}, u32[]{:S(2)}) %collective-permute-start.3) | collective-permute-done | bytes 2097184 | tf_op jit(solution)/shard_map/ppermute | solution.py:16
  119.3 1.7 constant_dynamic-update-slice_fusion.4
  121.3 2.0 copy-done.1
  123.3 1.7 reshape.557
  125.0 3.9 %fusion.4 = (f32[4,8,64]{2,1,0:T(8,128)S(1)}, f32[4,8,64,192]{3,2,1,0:T(8,128)}) fusion(pred[4,64,192]{2,1,0:T(8,128)(4,1)S(1)} %broadcast_and_fusion.1, bf16[192,4,8,64]{3,2,1,0:T(8,128)(2,1)} %reshape.557, bf16[64,4,8,64]{3,2,1,0:T(8,128)(2,1)S(1)} %bitcast.131), kind=kOutput, calls=%fused_computation.14 | convolution fusion | flops 51509248 | bytes 2678784 | tf_op jit(solution)/shard_map/qrhc,krhc->rhqk/dot_general | solution.py:48
  130.7 2.5 %fusion.7 = f32[4,8,64]{2,1,0:T(8,128)S(1)} fusion(f32[4,8,64,192]{3,2,1,0:T(8,128)} %get-tuple-element.30, f32[4,8,64]{2,1,0:T(8,128)S(1)} %get-tuple-element.29, pred[4,64,192]{2,1,0:T(8,128)(4,1)S(1)} %broadcast_and_fusion.1), kind=kLoop, calls=%fused_computation.17 | loop fusion | flops 1570816 | bytes 1638400 | tf_op jit(solution)/shard_map/reduce_sum | solution.py:62
  134.0 3.6 %fusion.28 = f32[64,4,8,64]{0,3,2,1:T(8,128)} fusion(bf16[192,4,8,64]{3,2,1,0:T(8,128)(2,1)} %reshape.564, f32[4,8,64,192]{3,2,1,0:T(8,128)S(1)} %copy-done.4, f32[4,8,64]{2,1,0:T(8,128)S(1)} %get-tuple-element.29, pred[4,64,192]{2,1,0:T(8,128)(4,1)S(1)} %broadcast_and_fusion.1, f32[64,4,8]{0,2,1:T(8,128)S(1)} %bitcast.146), kind=kOutput, calls=%fused_computation.32 | convolution fusion | flops 52297728 | bytes 2949120 | tf_op jit(solution)/shard_map/rhqk,krhc->qrhc/dot_general | solution.py:63
  137.6 2.1 %copy.160 = f32[64,4,8,64]{3,2,1,0:T(8,128)S(1)} copy(f32[64,4,8,64]{0,3,2,1:T(8,128)} %fusion.28) | data formatting | bytes 1048576 | tf_op jit(solution)/shard_map/convert_element_type | solution.py:110
  141.0 3.9 %slice_bitcast_fusion = (bf16[2048,512]{1,0:T(8,128)(2,1)}, bf16[2048,512]{1,0:T(8,128)(2,1)S(1)}) fusion(bf16[2,2048,512]{2,1,0:T(8,128)(2,1)} %copy-done.1), kind=kLoop, calls=%fused_computation.7 | loop fusion | bytes 8388608 | tf_op jit(solution)/shard_map/squeeze | solution.py:100
  145.0 4.3 %reshape.559 = bf16[144,16,8,64]{3,2,1,0:T(8,128)(2,1)} reshape(bf16[2304,512]{1,0:T(8,128)(2,1)S(1)} %pad_maximum_fusion) | data formatting | bytes 4718592 | tf_op jit(solution)/shard_map/reshape | solution.py:40
  149.3 1.7 pad_maximum_fusion.1
  151.1 4.4 %reshape.566 = bf16[144,16,8,64]{3,2,1,0:T(8,128)(2,1)} reshape(bf16[2304,512]{1,0:T(8,128)(2,1)S(1)} %pad_maximum_fusion.1) | data formatting | bytes 4718592 | tf_op jit(solution)/shard_map/reshape | solution.py:41
  155.5 7.2 %fusion.5 = (f32[16,8,16]{2,1,0:T(8,128)S(1)}, f32[16,8,16,144]{3,2,1,0:T(8,128)S(1)}) fusion(pred[16,16,144]{2,1,0:T(8,128)(4,1)S(1)} %broadcast_and_fusion, bf16[144,16,8,64]{3,2,1,0:T(8,128)(2,1)} %reshape.559, bf16[16,16,8,64]{3,2,1,0:T(8,128)(2,1)S(1)} %bitcast.132), kind=kOutput, calls=%fused_computation.15 | convolution fusion | flops 38631424 | bytes 3846144 | tf_op jit(solution)/shard_map/qrhc,krhc->rhqk/dot_general | solution.py:48
  163.6 6.6 %fusion.53 = f32[16,16,8,64]{3,0,2,1:T(8,128)S(1)} fusion(bf16[144,16,8,64]{3,2,1,0:T(8,128)(2,1)} %reshape.566, f32[16,8,16,144]{3,2,1,0:T(8,128)S(1)} %get-tuple-element.32, f32[16,8,16]{2,1,0:T(8,128)S(1)} %get-tuple-element.31, pred[16,16,144]{2,1,0:T(8,128)(4,1)S(1)} %broadcast_and_fusion, f32[16,16,8]{0,2,1:T(8,128)S(1)} %bitcast.141), kind=kOutput, calls=%fused_computation.55 | convolution fusion | flops 39321600 | bytes 4116480 | tf_op jit(solution)/shard_map/rhqk,krhc->qrhc/dot_general | solution.py:63
  175.4 2.1 %mul.226 = f32[2,128,512]{1,0,2:T(2,128)} reshape(f32[256,8,64]{0,2,1:T(8,128)} %mul.225) | data formatting | bytes 1048576 | tf_op jit(solution)/shard_map/mul | solution.py:111
  177.5 1.8 fusion.64
  179.3 6.0 %all_to_all.16 = bf16[2,128,512]{1,2,0:T(8,128)(2,1)S(1)} all-to-all(bf16[2,128,512]{1,2,0:T(8,128)(2,1)S(1)} %copy.166), channel_id=1, replica_groups=mesh['sp'=256,'tp'=2] {'tp'}, dimensions={0} | all-to-all | bytes 524288 | tf_op jit(solution)/shard_map/all_to_all | solution.py:116
  185.3 3.7 %convolution_convert_fusion = bf16[128,2048]{1,0:T(8,128)(2,1)} fusion(bf16[128,1024]{0,1:T(8,128)(2,1)S(1)} %bitcast.135, bf16[1024,2048]{1,0:T(8,128)(2,1)} %all-gather.2.cloned.1.call-done), kind=kOutput, calls=%fused_computation.4 | convolution fusion | flops 537133056 | bytes 4980736 | tf_op jit(solution)/shard_map/dot_general | solution.py:117
  (107 shorter events, 28.5 us)
Async XLA Ops:
  6.5 178.7 %all-gather.2.cloned.1.call-start = ((), (), s32[]{:S(2)}) async-start(), calls=%async_computation.1 | async-start | bytes 6291456 | tf_op jit(solution)/shard_map/all_gather | solution.py:119
  7.7 1.7 copy-start
  10.2 15.0 %collective-permute-start = (bf16[2,256,512]{2,1,0:T(8,128)(2,1)}, bf16[2,256,512]{2,1,0:T(8,128)(2,1)S(1)}, u32[]{:S(2)}, u32[]{:S(2)}) collective-permute-start(bf16[2,256,512]{2,1,0:T(8,128)(2,1)} %pad_maximum_fusion.4), channel_id=1, source_target_pairs={{0,2},{2,4},{4,6},{6,8},{8,10},{10,12},{12,14},{14,16},{16,18},{18... | collective-permute-start | bytes 1572872 | tf_op jit(solution)/shard_map/ppermute | solution.py:16
  13.3 65.7 %collective-permute-start.2 = (bf16[2,256,512]{2,1,0:T(8,128)(2,1)}, bf16[2,256,512]{2,1,0:T(8,128)(2,1)}, u32[]{:S(2)}, u32[]{:S(2)}) collective-permute-start(bf16[2,256,512]{2,1,0:T(8,128)(2,1)} %pad_maximum_fusion.4), channel_id=1, source_target_pairs={{0,16},{2,18},{4,20},{6,22},{8,24},{10,26},{12,28},{14,30},{16,32}... | collective-permute-start | bytes 1572872 | tf_op jit(solution)/shard_map/ppermute | solution.py:16
  25.3 41.4 %collective-permute-start.1 = (bf16[2,512,512]{2,1,0:T(8,128)(2,1)S(1)}, bf16[2,512,512]{2,1,0:T(8,128)(2,1)S(1)}, u32[]{:S(2)}, u32[]{:S(2)}) collective-permute-start(bf16[2,512,512]{2,1,0:T(8,128)(2,1)S(1)} %maximum_maximum_fusion.1), channel_id=1, source_target_pairs={{0,4},{2,6},{4,8},{6,10},{8,12},{10,14},{12,16},{14,18},{16,20},{1... | collective-permute-start | bytes 3145736 | tf_op jit(solution)/shard_map/ppermute | solution.py:16
  29.5 40.6 %copy-start.9 = (f32[8,128]{1,0:T(8,128)}, f32[8,128]{1,0:T(8,128)S(1)}, u32[]{:S(2)}) copy-start(f32[8,128]{1,0:T(8,128)S(1)} %get-tuple-element.33) | copy-start | bytes 12292
  29.9 40.2 %copy-start.13 = (f32[8,128]{1,0:T(8,128)}, f32[8,128]{1,0:T(8,128)S(1)}, u32[]{:S(2)}) copy-start(f32[8,128]{1,0:T(8,128)S(1)} %fusion.48) | copy-start | bytes 12292
  30.1 40.0 %copy-start.6 = (bf16[256,512]{0,1:T(8,128)(2,1)S(1)}, bf16[256,512]{0,1:T(8,128)(2,1)}, u32[]{:S(2)}) copy-start(bf16[256,512]{0,1:T(8,128)(2,1)} %copy.155) | copy-start | bytes 786436
  68.1 51.2 %collective-permute-start.3 = (bf16[2,1024,512]{2,1,0:T(8,128)(2,1)}, bf16[2,1024,512]{2,1,0:T(8,128)(2,1)}, u32[]{:S(2)}, u32[]{:S(2)}) collective-permute-start(bf16[2,1024,512]{2,1,0:T(8,128)(2,1)} %maximum_maximum_fusion), channel_id=1, source_target_pairs={{0,8},{2,10},{4,12},{6,14},{8,16},{10,18},{12,20},{14,22},{16,24},... | collective-permute-start | bytes 6291464 | tf_op jit(solution)/shard_map/ppermute | solution.py:16
  74.4 3.2 %copy-start.7 = (bf16[256,512]{0,1:T(8,128)(2,1)S(1)}, bf16[256,512]{0,1:T(8,128)(2,1)}, u32[]{:S(2)}) copy-start(bf16[256,512]{0,1:T(8,128)(2,1)} %copy.154) | copy-start | bytes 786436
  75.3 2.6 %copy-start.8 = (bf16[128,1,8,64]{0,3,2,1:T(8,128)(2,1)S(1)}, bf16[128,1,8,64]{0,3,2,1:T(8,128)(2,1)}, u32[]{:S(2)}) copy-start(bf16[128,1,8,64]{0,3,2,1:T(8,128)(2,1)} %fusion.34) | copy-start | bytes 393220
  76.6 1.4 copy-start.11
  77.0 0.6 copy-start.15
  121.2 2.0 %copy-start.1 = (bf16[2,2048,512]{2,1,0:T(8,128)(2,1)}, bf16[2,2048,512]{2,1,0:T(8,128)(2,1)S(1)}, u32[]{:S(2)}) copy-start(bf16[2,2048,512]{2,1,0:T(8,128)(2,1)S(1)} %get-tuple-element.21) | copy-start | bytes 12582916
  130.7 3.3 %copy-start.4 = (f32[4,8,64,192]{3,2,1,0:T(8,128)S(1)}, f32[4,8,64,192]{3,2,1,0:T(8,128)}, u32[]{:S(2)}) copy-start(f32[4,8,64,192]{3,2,1,0:T(8,128)} %get-tuple-element.30) | copy-start | bytes 4718596
  170.3 1.2 copy-start.5
  170.6 1.1 copy-start.10
  170.6 1.1 copy-start.12
  170.6 1.1 copy-start.14
  170.7 1.1 copy-start.16
  172.1 5.4 %copy-start.2 = (f32[2,128,512]{1,0,2:T(2,128)S(1)}, f32[2,128,512]{1,0,2:T(2,128)}, u32[]{:S(2)}) copy-start(f32[2,128,512]{1,0,2:T(2,128)} %reshape.571) | copy-start | bytes 1572868
  172.1 5.4 %copy-start.3 = (f32[2,128,512]{1,0,2:T(2,128)S(1)}, f32[2,128,512]{1,0,2:T(2,128)}, u32[]{:S(2)}) copy-start(f32[2,128,512]{1,0,2:T(2,128)} %copy.161) | copy-start | bytes 1572868
Sparse Core Ops, SparseCore 0:
  18.3 24.7 all-gather.1
where the time goes:
time: 197 us; the launch traced here: 196 us
  waiting for transfers between devices  80.6 us (41%)
  local copies, waits for them, and re-layouts  39.9 us (20%)
  matrix products  28.1 us (14%)
  between operations  14 us (7%)
  other arithmetic  13.7 us (7%)
  starting transfers between devices  13.6 us (7%)
  blocking collectives  5.97 us (3%)
    ppermute x4, waiting for transfers between devices, shifted(): lax.ppermute(value, axis, [(source, source + steps) for source in range(i...  80.6 us
    ppermute x4, starting transfers between devices, shifted(): lax.ppermute(value, axis, [(source, source + steps) for source in range(i...  13.6 us
    dot_general x4, matrix products, pattern_part(): jnp.einsum('qrhc,krhc->rhqk', query_sub[first_row:first_row + block_rows]...  12.7 us
    dot_general x4, matrix products, pattern_part(): jnp.einsum('rhqk,krhc->qrhc', weights.astype(jnp.bfloat16), value_part, p...  11.6 us
    unnamed x38, local copies, waits for them, and re-layouts  6.39 us
    reshape x2, local copies, waits for them, and re-layouts, pattern_part(): value_sub = value_ext.reshape(BACK + length, dilation, head_count, HD)  6.09 us
    reshape x2, local copies, waits for them, and re-layouts, pattern_part(): key_sub = key_ext.reshape(BACK + length, dilation, head_count, HD)  6.02 us
    all_to_all x1, blocking collectives, per_device(): lax.all_to_all(mixed, 'tp', split_axis=0, concat_axis=1, tiled=True)  5.97 us
  transfers between devices with their start and end apart: 5, of which 3 were waited for; matrix products, arithmetic and copies ran while one was open for 37% of the time, Pallas kernels for 0%

commit v1 on v0

--- a/solution.py
+++ b/solution.py
@@ -113,7 +113,9 @@
     mixed = (
         (weighted / denominator[..., None]).reshape(tok_rows, head_count * HD).astype(jnp.bfloat16)
     )
-    token_rows = lax.all_to_all(mixed, "tp", split_axis=0, concat_axis=1, tiled=True)
+    token_rows = jnp.concatenate(
+        lax.all_to_all(jnp.stack(jnp.split(mixed, lax.axis_size("tp"), axis=0)), "tp", 0, 0), axis=1
+    )
     projected = jnp.dot(
         token_rows,
         lax.all_gather(out_weight, "tp", axis=0, tiled=True),

time: 197 us -> 190 us (0.964)
  local copies, waits for them, and re-layouts: 39.9 us -> 36.1 us
    mul x6 -> x0, local copies, waits for them, and re-layouts: 5.37 us -> none  [the longest x2 2.93 us: per_device(): weighted = weighted + scales[2][..., None] * results[2].astype(jnp.float32)]
    squeeze x1 -> x4, local copies, waits for them, and re-layouts: 0.77 us -> 6.11 us  [per_device(): prior[0, prior.shape[1] - reach:]]
    squeeze x3 -> x0, local copies, waits for them, and re-layouts: 4.59 us -> none  [per_device(): prior[1, prior.shape[1] - reach:]]
    dot_general x4, matrix products: 12.7 us -> 10 us  [pattern_part(): jnp.einsum('qrhc,krhc->rhqk', query_sub[first_row:first_row + block_rows]...]
    unnamed x38 -> x52, local copies, waits for them, and re-layouts: 6.39 us -> 8.55 us
  transfers between devices with their start and end apart: 5 -> 5, of which waited for: 3 -> 3; matrix products, arithmetic and copies ran while one was open for 37% -> 33% of each run, Pallas kernels for 0% -> 0%
where the time goes in v1:
time: 190 us
  waiting for transfers between devices  81.4 us (43%)
  local copies, waits for them, and re-layouts  36.1 us (19%)
  matrix products  26.3 us (14%)
  between operations  14 us (7%)
  starting transfers between devices  13.8 us (7%)
  other arithmetic  12.3 us (6%)
  blocking collectives  5.97 us (3%)
    ppermute x4, waiting for transfers between devices, shifted(): lax.ppermute(value, axis, [(source, source + steps) for source in range(i...  81.4 us
    ppermute x4, starting transfers between devices, shifted(): lax.ppermute(value, axis, [(source, source + steps) for source in range(i...  13.8 us
    dot_general x4, matrix products, pattern_part(): jnp.einsum('rhqk,krhc->qrhc', weights.astype(jnp.bfloat16), value_part, p...  12.6 us
    dot_general x4, matrix products, pattern_part(): jnp.einsum('qrhc,krhc->rhqk', query_sub[first_row:first_row + block_rows]...  10 us
    unnamed x52, local copies, waits for them, and re-layouts  8.55 us
    squeeze x4, local copies, waits for them, and re-layouts, per_device(): prior[0, prior.shape[1] - reach:]  6.11 us
    reshape x2, local copies, waits for them, and re-layouts, pattern_part(): value_sub = value_ext.reshape(BACK + length, dilation, head_count, HD)  6.06 us
    all_to_all x1, blocking collectives, per_device(): lax.all_to_all(jnp.stack(jnp.split(mixed, lax.axis_size('tp'), axis=0)),...  5.97 us
  transfers between devices with their start and end apart: 5, of which 3 were waited for; matrix products, arithmetic and copies ran while one was open for 33% of the time, Pallas kernels for 0%

profile of v1, /device:TPU:259, one launch (start us, length us, event | category | flops | bytes accessed | tf_op | source)
XLA Modules:
  0.0 189.8 jit_solution(17181516302657742752)
XLA Ops:
  10.2 3.1 %collective-permute-start = (bf16[2,256,512]{2,1,0:T(8,128)(2,1)}, bf16[2,256,512]{2,1,0:T(8,128)(2,1)S(1)}, u32[]{:S(2)}, u32[]{:S(2)}) collective-permute-start(bf16[2,256,512]{2,1,0:T(8,128)(2,1)} %pad_maximum_fusion.4), channel_id=1, source_target_pairs={{0,2},{2,4},{4,6},{6,8},{8,10},{10,12},{12,14},{14,16},{16,18},{18... | collective-permute-start | bytes 1572872 | tf_op jit(solution)/shard_map/ppermute | solution.py:16
  13.3 4.8 %collective-permute-start.2 = (bf16[2,256,512]{2,1,0:T(8,128)(2,1)}, bf16[2,256,512]{2,1,0:T(8,128)(2,1)}, u32[]{:S(2)}, u32[]{:S(2)}) collective-permute-start(bf16[2,256,512]{2,1,0:T(8,128)(2,1)} %pad_maximum_fusion.4), channel_id=1, source_target_pairs={{0,16},{2,18},{4,20},{6,22},{8,24},{10,26},{12,28},{14,30},{16,32}... | collective-permute-start | bytes 1572872 | tf_op jit(solution)/shard_map/ppermute | solution.py:16
  20.3 4.9 %collective-permute-done = bf16[2,256,512]{2,1,0:T(8,128)(2,1)S(1)} collective-permute-done((bf16[2,256,512]{2,1,0:T(8,128)(2,1)}, bf16[2,256,512]{2,1,0:T(8,128)(2,1)S(1)}, u32[]{:S(2)}, u32[]{:S(2)}) %collective-permute-start) | collective-permute-done | bytes 524320 | tf_op jit(solution)/shard_map/ppermute | solution.py:16
  25.3 3.8 %collective-permute-start.1 = (bf16[2,512,512]{2,1,0:T(8,128)(2,1)S(1)}, bf16[2,512,512]{2,1,0:T(8,128)(2,1)S(1)}, u32[]{:S(2)}, u32[]{:S(2)}) collective-permute-start(bf16[2,512,512]{2,1,0:T(8,128)(2,1)S(1)} %maximum_maximum_fusion.1), channel_id=1, source_target_pairs={{0,4},{2,6},{4,8},{6,10},{8,12},{10,14},{12,16},{14,18},{16,20},{1... | collective-permute-start | bytes 3145736 | tf_op jit(solution)/shard_map/ppermute | solution.py:16
  30.1 36.6 %collective-permute-done.1 = bf16[2,512,512]{2,1,0:T(8,128)(2,1)S(1)} collective-permute-done((bf16[2,512,512]{2,1,0:T(8,128)(2,1)S(1)}, bf16[2,512,512]{2,1,0:T(8,128)(2,1)S(1)}, u32[]{:S(2)}, u32[]{:S(2)}) %collective-permute-start.1) | collective-permute-done | bytes 1048608 | tf_op jit(solution)/shard_map/ppermute | solution.py:16
  66.6 1.5 maximum_maximum_fusion
  68.1 2.1 %collective-permute-start.3 = (bf16[2,1024,512]{2,1,0:T(8,128)(2,1)}, bf16[2,1024,512]{2,1,0:T(8,128)(2,1)}, u32[]{:S(2)}, u32[]{:S(2)}) collective-permute-start(bf16[2,1024,512]{2,1,0:T(8,128)(2,1)} %maximum_maximum_fusion), channel_id=1, source_target_pairs={{0,8},{2,10},{4,12},{6,14},{8,16},{10,18},{12,20},{14,22},{16,24},... | collective-permute-start | bytes 6291464 | tf_op jit(solution)/shard_map/ppermute | solution.py:16
  79.4 39.9 %collective-permute-done.3 = bf16[2,1024,512]{2,1,0:T(8,128)(2,1)} collective-permute-done((bf16[2,1024,512]{2,1,0:T(8,128)(2,1)}, bf16[2,1024,512]{2,1,0:T(8,128)(2,1)}, u32[]{:S(2)}, u32[]{:S(2)}) %collective-permute-start.3) | collective-permute-done | bytes 2097184 | tf_op jit(solution)/shard_map/ppermute | solution.py:16
  119.3 1.7 constant_dynamic-update-slice_fusion.4
  121.3 1.9 %copy-done.2 = bf16[2,2048,512]{2,1,0:T(8,128)(2,1)} copy-done((bf16[2,2048,512]{2,1,0:T(8,128)(2,1)}, bf16[2,2048,512]{2,1,0:T(8,128)(2,1)S(1)}, u32[]{:S(2)}) %copy-start.2) | copy-done | bytes 4194328
  125.0 1.2 fusion.4
  126.2 1.3 copy-done.3
  129.1 3.8 %slice_bitcast_fusion.1 = (bf16[2048,512]{1,0:T(8,128)(2,1)S(1)}, bf16[2048,512]{1,0:T(8,128)(2,1)}) fusion(bf16[2,2048,512]{2,1,0:T(8,128)(2,1)} %copy-done.2), kind=kLoop, calls=%fused_computation.8 | loop fusion | bytes 8388608 | tf_op jit(solution)/shard_map/squeeze | solution.py:99
  133.1 4.3 %reshape.555 = bf16[144,16,8,64]{3,2,1,0:T(8,128)(2,1)} reshape(bf16[2304,512]{1,0:T(8,128)(2,1)S(1)} %pad_maximum_fusion) | data formatting | bytes 4718592 | tf_op jit(solution)/shard_map/reshape | solution.py:40
  137.4 7.2 %fusion.5 = (f32[16,8,16]{2,1,0:T(8,128)S(1)}, f32[16,8,16,144]{3,2,1,0:T(8,128)S(1)}) fusion(pred[16,16,144]{2,1,0:T(8,128)(4,1)S(1)} %broadcast_and_fusion, bf16[144,16,8,64]{3,2,1,0:T(8,128)(2,1)} %reshape.555, bf16[16,16,8,64]{3,2,1,0:T(8,128)(2,1)S(1)} %bitcast.147), kind=kOutput, calls=%fused_computation.15 | convolution fusion | flops 38631424 | bytes 3846144 | tf_op jit(solution)/shard_map/qrhc,krhc->rhqk/dot_general | solution.py:48
  144.6 1.4 copy-done.1
  150.5 1.7 reshape.560
  152.2 3.6 %fusion.28 = f32[64,4,8,64]{0,3,2,1:T(8,128)} fusion(bf16[192,4,8,64]{3,2,1,0:T(8,128)(2,1)} %reshape.560, f32[4,8,64,192]{3,2,1,0:T(8,128)S(1)} %copy-done.4, f32[4,8,64]{2,1,0:T(8,128)S(1)} %get-tuple-element.33, pred[4,64,192]{2,1,0:T(8,128)(4,1)S(1)} %copy-done.7, f32[64,4,8]{0,2,1:T(8,128)} %bitcast.161), kind=kOutput, calls=%fused_computation.32 | convolution fusion | flops 52297728 | bytes 2949120 | tf_op jit(solution)/shard_map/rhqk,krhc->qrhc/dot_general | solution.py:63
  155.8 2.1 %copy.156 = f32[64,4,8,64]{3,2,1,0:T(8,128)S(1)} copy(f32[64,4,8,64]{0,3,2,1:T(8,128)} %fusion.28) | data formatting | bytes 1048576 | tf_op jit(solution)/shard_map/convert_element_type | solution.py:110
  158.4 1.7 pad_maximum_fusion.1
  160.1 4.3 %reshape.562 = bf16[144,16,8,64]{3,2,1,0:T(8,128)(2,1)} reshape(bf16[2304,512]{1,0:T(8,128)(2,1)S(1)} %pad_maximum_fusion.1) | data formatting | bytes 4718592 | tf_op jit(solution)/shard_map/reshape | solution.py:41
  164.5 7.6 %fusion.53 = f32[16,16,8,64]{3,0,2,1:T(8,128)S(1)} fusion(bf16[144,16,8,64]{3,2,1,0:T(8,128)(2,1)} %reshape.562, f32[16,8,16,144]{3,2,1,0:T(8,128)} %copy-done.1, f32[16,8,16]{2,1,0:T(8,128)S(1)} %get-tuple-element.31, pred[16,16,144]{2,1,0:T(8,128)(4,1)S(1)} %broadcast_and_fusion, f32[16,16,8]{0,2,1:T(8,128)S(1)} %bitcast.156), kind=kOutput, calls=%fused_computation.55 | convolution fusion | flops 39321600 | bytes 4116480 | tf_op jit(solution)/shard_map/rhqk,krhc->qrhc/dot_general | solution.py:63
  173.3 6.0 %all_to_all.5 = bf16[2,128,512]{1,2,0:T(8,128)(2,1)S(1)} all-to-all(bf16[2,128,512]{1,2,0:T(8,128)(2,1)S(1)} %pad_maximum_fusion.8), channel_id=1, replica_groups=mesh['sp'=256,'tp'=2] {'tp'}, dimensions={0} | all-to-all | bytes 524288 | tf_op jit(solution)/shard_map/all_to_all | solution.py:117
  179.3 3.7 %convolution_convert_fusion = bf16[128,2048]{1,0:T(8,128)(2,1)} fusion(bf16[128,1024]{0,1:T(8,128)(2,1)S(1)} %bitcast.150, bf16[1024,2048]{1,0:T(8,128)(2,1)} %all-gather.2.cloned.1.call-done), kind=kOutput, calls=%fused_computation.4 | convolution fusion | flops 537133056 | bytes 4980736 | tf_op jit(solution)/shard_map/dot_general | solution.py:119
  (113 shorter events, 25.5 us)
Async XLA Ops:
  6.5 172.7 %all-gather.2.cloned.1.call-start = ((), (), s32[]{:S(2)}) async-start(), calls=%async_computation.1 | async-start | bytes 6291456 | tf_op jit(solution)/shard_map/all_gather | solution.py:121
  7.7 1.7 copy-start
  10.2 15.0 %collective-permute-start = (bf16[2,256,512]{2,1,0:T(8,128)(2,1)}, bf16[2,256,512]{2,1,0:T(8,128)(2,1)S(1)}, u32[]{:S(2)}, u32[]{:S(2)}) collective-permute-start(bf16[2,256,512]{2,1,0:T(8,128)(2,1)} %pad_maximum_fusion.4), channel_id=1, source_target_pairs={{0,2},{2,4},{4,6},{6,8},{8,10},{10,12},{12,14},{14,16},{16,18},{18... | collective-permute-start | bytes 1572872 | tf_op jit(solution)/shard_map/ppermute | solution.py:16
  13.3 65.0 %collective-permute-start.2 = (bf16[2,256,512]{2,1,0:T(8,128)(2,1)}, bf16[2,256,512]{2,1,0:T(8,128)(2,1)}, u32[]{:S(2)}, u32[]{:S(2)}) collective-permute-start(bf16[2,256,512]{2,1,0:T(8,128)(2,1)} %pad_maximum_fusion.4), channel_id=1, source_target_pairs={{0,16},{2,18},{4,20},{6,22},{8,24},{10,26},{12,28},{14,30},{16,32}... | collective-permute-start | bytes 1572872 | tf_op jit(solution)/shard_map/ppermute | solution.py:16
  25.3 41.4 %collective-permute-start.1 = (bf16[2,512,512]{2,1,0:T(8,128)(2,1)S(1)}, bf16[2,512,512]{2,1,0:T(8,128)(2,1)S(1)}, u32[]{:S(2)}, u32[]{:S(2)}) collective-permute-start(bf16[2,512,512]{2,1,0:T(8,128)(2,1)S(1)} %maximum_maximum_fusion.1), channel_id=1, source_target_pairs={{0,4},{2,6},{4,8},{6,10},{8,12},{10,14},{12,16},{14,18},{16,20},{1... | collective-permute-start | bytes 3145736 | tf_op jit(solution)/shard_map/ppermute | solution.py:16
  29.5 40.8 %copy-start.12 = (f32[8,128]{1,0:T(8,128)}, f32[8,128]{1,0:T(8,128)S(1)}, u32[]{:S(2)}) copy-start(f32[8,128]{1,0:T(8,128)S(1)} %get-tuple-element.35) | copy-start | bytes 12292
  29.9 40.4 %copy-start.20 = (f32[8,128]{1,0:T(8,128)}, f32[8,128]{1,0:T(8,128)S(1)}, u32[]{:S(2)}) copy-start(f32[8,128]{1,0:T(8,128)S(1)} %fusion.48) | copy-start | bytes 12292
  30.1 40.2 %copy-start.8 = (bf16[256,512]{0,1:T(8,128)(2,1)S(1)}, bf16[256,512]{0,1:T(8,128)(2,1)}, u32[]{:S(2)}) copy-start(bf16[256,512]{0,1:T(8,128)(2,1)} %copy.151) | copy-start | bytes 786436
  68.1 51.2 %collective-permute-start.3 = (bf16[2,1024,512]{2,1,0:T(8,128)(2,1)}, bf16[2,1024,512]{2,1,0:T(8,128)(2,1)}, u32[]{:S(2)}, u32[]{:S(2)}) collective-permute-start(bf16[2,1024,512]{2,1,0:T(8,128)(2,1)} %maximum_maximum_fusion), channel_id=1, source_target_pairs={{0,8},{2,10},{4,12},{6,14},{8,16},{10,18},{12,20},{14,22},{16,24},... | collective-permute-start | bytes 6291464 | tf_op jit(solution)/shard_map/ppermute | solution.py:16
  70.3 55.9 %copy-start.6 = (pred[4,64,192]{2,1,0:T(8,128)(4,1)}, pred[4,64,192]{2,1,0:T(8,128)(4,1)S(1)}, u32[]{:S(2)}) copy-start(pred[4,64,192]{2,1,0:T(8,128)(4,1)S(1)} %broadcast_and_fusion.1) | copy-start | bytes 147460
  74.6 2.6 %copy-start.9 = (bf16[256,512]{0,1:T(8,128)(2,1)S(1)}, bf16[256,512]{0,1:T(8,128)(2,1)}, u32[]{:S(2)}) copy-start(bf16[256,512]{0,1:T(8,128)(2,1)} %copy.150) | copy-start | bytes 786436
  75.5 2.0 %copy-start.10 = (bf16[128,1,8,64]{0,3,2,1:T(8,128)(2,1)S(1)}, bf16[128,1,8,64]{0,3,2,1:T(8,128)(2,1)}, u32[]{:S(2)}) copy-start(bf16[128,1,8,64]{0,3,2,1:T(8,128)(2,1)} %fusion.34) | copy-start | bytes 393220
  76.8 2.6 %copy-start.14 = (f32[8,128]{1,0:T(8,128)}, f32[8,128]{1,0:T(8,128)S(1)}, u32[]{:S(2)}) copy-start(f32[8,128]{1,0:T(8,128)S(1)} %get-tuple-element.37) | copy-start | bytes 12292
  77.2 43.9 %copy-start.22 = (f32[8,128]{1,0:T(8,128)}, f32[8,128]{1,0:T(8,128)S(1)}, u32[]{:S(2)}) copy-start(f32[8,128]{1,0:T(8,128)S(1)} %fusion.46) | copy-start | bytes 12292
  121.3 1.9 %copy-start.2 = (bf16[2,2048,512]{2,1,0:T(8,128)(2,1)}, bf16[2,2048,512]{2,1,0:T(8,128)(2,1)S(1)}, u32[]{:S(2)}) copy-start(bf16[2,2048,512]{2,1,0:T(8,128)(2,1)S(1)} %get-tuple-element.22) | copy-start | bytes 12582916
  126.2 1.3 copy-start.3
  128.3 4.6 %copy-start.11 = (f32[4,8,64]{2,1,0:T(8,128)}, f32[4,8,64]{2,1,0:T(8,128)S(1)}, u32[]{:S(2)}) copy-start(f32[4,8,64]{2,1,0:T(8,128)S(1)} %fusion.7) | copy-start | bytes 24580
  144.6 1.4 copy-start.1
  148.6 3.6 %copy-start.4 = (f32[4,8,64,192]{3,2,1,0:T(8,128)S(1)}, f32[4,8,64,192]{3,2,1,0:T(8,128)}, u32[]{:S(2)}) copy-start(f32[4,8,64,192]{3,2,1,0:T(8,128)} %copy-done.3) | copy-start | bytes 4718596
  148.6 3.6 %copy-start.7 = (pred[4,64,192]{2,1,0:T(8,128)(4,1)S(1)}, pred[4,64,192]{2,1,0:T(8,128)(4,1)}, u32[]{:S(2)}) copy-start(pred[4,64,192]{2,1,0:T(8,128)(4,1)} %copy-done.6) | copy-start | bytes 147460
  172.0 0.9 copy-start.16
  172.1 0.9 copy-start.17
  172.1 0.9 copy-start.18
  172.1 1.0 copy-start.5
  (5 other events, 4.6 us)
Sparse Core Ops, SparseCore 0:
  18.3 24.7 all-gather.1
